TPU v7x, 256 devices: a 4x2x16 block of a 4x16x16 slice. The times are simulated.
256 devices in a mesh: grp: 2 (over y), sp: 16 (over z), tp: 8 (over x, core).
Axes of the slice: x: 4, y: 2, z: 16, core: 2. Of those that a mesh axis runs over, the one named last changes fastest.
The devices are a block of a 4x16x16 slice.
Arguments:
- queries: bfloat16 [24576, 1024], P(('grp', 'sp'), 'tp'), parts along dimension 0, may hold values from -8 to 8
- keys: bfloat16 [24576, 256], P(('grp', 'sp')), parts along dimension 0, may hold values from -8 to 8
- values: bfloat16 [24576, 256], P(('grp', 'sp')), parts along dimension 0, may hold values from -6 to 6
- query_gain: float32 [128], replicated, may hold values from 0.2 to 6
- key_gain: float32 [128], replicated, may hold values from 0.2 to 6
- residual: bfloat16 [24576, 2048], P(('grp', 'sp', 'tp')), parts along dimension 0, may hold values from -6 to 6
- out_weight: bfloat16 [1024, 2048], P('tp'), may hold values from -0.1875 to 0.1875
- mix_gain: float32 [2048], replicated, may hold values from 0.1 to 1.9
- ffn_gain: float32 [2048], replicated, may hold values from 0.1 to 1.9
- gate_in: bfloat16 [2048, 5632], P('sp', 'tp'), may hold values from -0.125 to 0.125
- value_in: bfloat16 [2048, 5632], P('sp', 'tp'), may hold values from -0.125 to 0.125
- conv_gate: float32 [3, 5632], P(None, 'tp'), may hold values from -3 to 3
- conv_value: float32 [3, 5632], P(None, 'tp'), may hold values from -3 to 3
- down_t: bfloat16 [2048, 5632], P('sp', 'tp'), may hold values from -0.078125 to 0.078125
Outputs:
- layer_out: bfloat16 [24576, 2048], P(('grp', 'sp', 'tp')), parts along dimension 0
There are 2 independent parts, one for each index of `grp`. A program takes and returns all parts, laid end to end along the dimension named above; an argument that names none is the same for every part. Nothing has to cross between parts.
All inputs are finite; a program needn't handle non-finite values.
Results may differ from a plain program's by a relative error of at most 0.02.
The roundings to bfloat16 on the way count: a program that leaves them out, or rounds other values in their place, can miss the bound.
Values may be sent and summed in bfloat16 or wider, within the bound.
A program may use at most 128 MiB of HBM per device.

v0:
```python
import jax
import jax.numpy as jnp
from jax import lax
from jax.sharding import PartitionSpec as P

HEADS = 8
KVH = 2
GRID_W = 64
EPSILON = 1e-06
THETA = 10000.0


def sent_together(arrays, axis, dim, along):
    both = jnp.concatenate(arrays, axis=along)
    whole, at, gathered = (lax.all_gather(both, axis, axis=dim, tiled=True), 0, [])
    for a in arrays:
        gathered.append(lax.slice_in_dim(whole, at, at + a.shape[along], axis=along))
        at += a.shape[along]
    return tuple(gathered)


def cut_along(array, dim, size):
    before, after = (array.shape[:dim], array.shape[dim + 1 :])
    return jnp.moveaxis(array.reshape(*before, size, -1, *after), dim, 0)


def summed_on_arrival(array, axis, dim):
    tiles = cut_along(array, dim, lax.axis_size(axis))
    arrived = lax.all_to_all(tiles, axis, split_axis=0, concat_axis=0, tiled=True)
    return arrived.astype(jnp.float32).sum(axis=0)


def with_halo(block, sides, width):
    for axis, dim in sides:
        count = lax.axis_size(axis)
        forward = [(i, i + 1) for i in range(count - 1)]
        backward = [(target, source) for source, target in forward]
        low = lax.ppermute(
            lax.slice_in_dim(block, block.shape[dim] - width, None, axis=dim), axis, forward
        )
        high = lax.ppermute(lax.slice_in_dim(block, 0, width, axis=dim), axis, backward)
        block = jnp.concatenate([low, block, high], axis=dim)
    return block


def rotary_tables(positions, seq_total, head_dim):
    quarter = head_dim // 4
    inverse = THETA ** (-(2.0 * jnp.arange(quarter, dtype=jnp.float32)) / (head_dim // 2))
    grid_row = (positions // GRID_W - seq_total // GRID_W // 2).astype(jnp.float32)
    grid_col = (positions % GRID_W - GRID_W // 2).astype(jnp.float32)
    row_angle = grid_row[:, None] * inverse[None, :]
    col_angle = grid_col[:, None] * inverse[None, :]
    angle = jnp.concatenate([row_angle, row_angle, col_angle, col_angle], axis=-1)
    return (jnp.cos(angle), jnp.sin(angle))


def rotate_quarters(vector):
    first, second, third, fourth = jnp.split(vector, 4, axis=-1)
    return jnp.concatenate([-second, first, -fourth, third], axis=-1)


def prepare_heads(raw, gain, cos_table, sin_table, factor):
    floats = raw.astype(jnp.float32)
    normed = floats * lax.rsqrt(jnp.mean(floats * floats, axis=-1, keepdims=True) + EPSILON) * gain
    turned = normed * cos_table + rotate_quarters(normed) * sin_table
    return (turned * factor).astype(jnp.bfloat16)


def rms_rows(stream, gain):
    floats = stream.astype(jnp.float32)
    return floats * lax.rsqrt(jnp.mean(floats * floats, axis=-1, keepdims=True) + EPSILON) * gain


def body(
    queries,
    keys,
    values,
    query_gain,
    key_gain,
    residual,
    out_weight,
    mix_gain,
    ffn_gain,
    gate_in,
    value_in,
    conv_gate,
    conv_value,
    down_t,
):
    gate_rows, value_rows, down_rows = sent_together((gate_in, value_in, down_t), "sp", 0, 1)
    tok_rows = queries.shape[0]
    head_dim = query_gain.shape[0]
    local_heads = queries.shape[1] // head_dim
    seq_total = tok_rows * lax.axis_size("sp")
    kv_head = lax.axis_index("tp") * local_heads // (HEADS // KVH)
    positions = lax.axis_index("sp") * tok_rows + jnp.arange(tok_rows, dtype=jnp.int32)
    cos_table, sin_table = rotary_tables(positions, seq_total, head_dim)
    key_own = lax.dynamic_slice_in_dim(keys, kv_head * head_dim, head_dim, 1)
    value_own = lax.dynamic_slice_in_dim(values, kv_head * head_dim, head_dim, 1)
    key_rot = prepare_heads(key_own, key_gain, cos_table, sin_table, 1.0)
    query_rot = prepare_heads(
        queries.reshape(tok_rows, local_heads, head_dim),
        query_gain,
        cos_table[:, None, :],
        sin_table[:, None, :],
        head_dim ** (-0.5),
    )
    query_rows = jnp.transpose(query_rot, (1, 0, 2)).reshape(local_heads * tok_rows, head_dim)
    query_count = local_heads * tok_rows
    running = jnp.full((query_count, 1), -1e30, jnp.float32)
    key_piece, value_piece = sent_together((key_rot, value_own), "sp", 0, 1)
    scores = lax.dot_general(
        query_rows, key_piece, (((1,), (1,)), ((), ())), preferred_element_type=jnp.float32
    )
    newest = jnp.maximum(running, jnp.max(scores, axis=1, keepdims=True))
    weights = jnp.exp(scores - newest)
    denom = jnp.sum(weights, axis=1, keepdims=True)
    summed = jnp.dot(weights.astype(jnp.bfloat16), value_piece, preferred_element_type=jnp.float32)
    running, denom, summed = (newest, denom, summed)
    attended = (summed / denom).astype(jnp.bfloat16).reshape(local_heads, tok_rows, head_dim)
    attended = jnp.transpose(attended, (1, 0, 2)).reshape(tok_rows, local_heads * head_dim)
    block_rows = attended
    mix = summed_on_arrival(
        jnp.dot(block_rows, out_weight, preferred_element_type=jnp.float32).astype(jnp.bfloat16),
        "tp",
        0,
    )
    stream = (residual.astype(jnp.float32) + rms_rows(mix, mix_gain)).astype(jnp.bfloat16)
    normed = rms_rows(stream, ffn_gain).astype(jnp.bfloat16)
    paired = jnp.concatenate([gate_rows, value_rows], axis=1)
    upward = jnp.dot(
        lax.all_gather(normed, "tp", axis=0, tiled=True), paired, preferred_element_type=jnp.float32
    ).astype(jnp.bfloat16)
    padded = with_halo(upward, (("sp", 0),), 1).astype(jnp.float32)
    taps = jnp.concatenate([conv_gate, conv_value], axis=1)
    mixed = taps[0] * padded[:-2] + taps[1] * padded[1:-1] + taps[2] * padded[2:]
    unit_cols = conv_gate.shape[1]
    hidden = (jax.nn.gelu(mixed[:, :unit_cols], approximate=True) * mixed[:, unit_cols:]).astype(
        jnp.bfloat16
    )
    block_rows = hidden
    ffn_out = summed_on_arrival(
        lax.dot_general(
            block_rows, down_rows, (((1,), (1,)), ((), ())), preferred_element_type=jnp.float32
        ).astype(jnp.bfloat16),
        "tp",
        0,
    )
    return (stream.astype(jnp.float32) + ffn_out).astype(jnp.bfloat16)


def solution(mesh):
    return jax.shard_map(
        body,
        mesh=mesh,
        in_specs=(
            P(("grp", "sp"), "tp"),
            P(("grp", "sp"), None),
            P(("grp", "sp"), None),
            P(),
            P(),
            P(("grp", "sp", "tp"), None),
            P("tp", None),
            P(),
            P(),
            P("sp", "tp"),
            P("sp", "tp"),
            P(None, "tp"),
            P(None, "tp"),
            P("sp", "tp"),
        ),
        out_specs=P(("grp", "sp", "tp"), None),
        check_vma=False,
    )
```

profile of v0, /device:TPU:33, one launch (start us, length us, event | category | flops | bytes accessed | tf_op | source)
XLA Modules:
  0.0 345.3 jit_solution(11012669087130800998)
XLA Ops:
  6.6 1.2 fusion.55
  7.8 1.1 fusion.56
  8.9 0.4 slice_negate_fusion.1
  9.3 0.9 constant_dynamic-slice_fusion
  10.3 0.3 broadcast_multiply_fusion.1
  10.6 2.0 fusion.60
  12.6 0.8 pad_maximum_fusion.2
  13.5 1.9 pad_maximum_fusion
  15.6 0.2 fusion.48
  15.8 0.2 fusion.50
  16.0 0.4 fusion.58
  16.3 93.2 %all-gather.4.cloned.1.call-done = bf16[12288,256]{1,0:T(8,128)(2,1)} async-done(((bf16[768,256]{1,0:T(8,128)(2,1)}), bf16[12288,256]{1,0:T(8,128)(2,1)}) %all-gather.4.cloned.1.call-update) | async-done | bytes 6291472 | tf_op jit(solution)/shard_map/all_gather | solution.py:15
  109.5 16.3 %fusion.87 = (f32[768]{0:T(1024)S(1)}, f32[768,12288]{1,0:T(8,128)}) fusion(bf16[12288,256]{1,0:T(8,128)(2,1)} %all-gather.4.cloned.1.call-done, bf16[768,128]{1,0:T(8,128)(2,1)S(1)} %copy-done.2, f32[768,32]{1,0:T(8,128)S(1)} %get-tuple-element.13, f32[768,32]{1,0:T(8,128)S(1)} %get-tuple-element.14, f32[768,32]{1,0:T(8,128)S(1)} %get-tuple-element.15, ...), kind=kOutput, calls=%fused_computation.117 | convolution fusion | flops 2426731776 | bytes 41687552 | tf_op jit(solution)/shard_map/dot_general | solution.py:112
  125.9 15.4 %fusion = f32[768]{0:T(1024)S(1)} fusion(f32[768,12288]{1,0:T(8,128)} %get-tuple-element.23, f32[768]{0:T(1024)S(1)} %broadcast_maximum_fusion), kind=kLoop, calls=%fused_computation.1 | loop fusion | flops 18873600 | bytes 37754880 | tf_op jit(solution)/shard_map/reduce_sum | solution.py:117
  141.2 18.7 %convolution_convert_fusion.1 = bf16[768,2048]{1,0:T(8,128)(2,1)} fusion(bf16[128,2048]{1,0:T(8,128)(2,1)S(1)} %copy-done, bf16[12288,256]{1,0:T(8,128)(2,1)} %all-gather.4.cloned.1.call-done, f32[768,12288]{1,0:T(8,128)} %get-tuple-element.23, f32[768]{0:T(1024)S(1)} %broadcast_maximum_fusion, f32[768]{0:T(1024)S(1)} %fusion), kind=kOutput, calls=%fused_computation.16 | convolution fusion | flops 2839216128 | bytes 44570624 | tf_op jit(solution)/shard_map/dot_general | solution.py:124
  159.9 45.7 %all_to_all.10 = bf16[8,96,2048]{2,1,0:T(8,128)(2,1)S(1)} all-to-all(bf16[8,96,2048]{2,1,0:T(8,128)(2,1)} %bitcast.14), channel_id=1, replica_groups=mesh['grp'=2,'sp'=16,'tp'=8] {'tp'}, dimensions={0} | all-to-all | bytes 6291456 | tf_op jit(solution)/shard_map/all_to_all | solution.py:29
  205.6 0.6 convert_reduce_fusion.1
  206.2 0.1 multiply_reduce_fusion
  206.3 0.3 fusion.44
  206.7 0.9 fusion.46
  207.7 22.5 %all-gather.8.cloned.1.call-done = bf16[2048,2112]{0,1:T(8,128)(2,1)} async-done(((bf16[128,2112]{0,1:T(8,128)(2,1)}), bf16[2048,2112]{0,1:T(8,128)(2,1)}) %all-gather.8.cloned.1.call-update) | async-done | bytes 8650768 | tf_op jit(solution)/shard_map/all_gather | solution.py:15
  230.2 42.3 %all-gather.6.cloned.1.call-done = bf16[768,2048]{1,0:T(8,128)(2,1)} async-done(((bf16[96,2048]{1,0:T(8,128)(2,1)}), bf16[768,2048]{1,0:T(8,128)(2,1)}) %all-gather.6.cloned.1.call-update) | async-done | bytes 3145744 | tf_op jit(solution)/shard_map/all_gather | solution.py:132
  272.5 8.4 %fusion.9 = bf16[768,1408]{1,0:T(8,128)(2,1)S(1)} fusion(bf16[768,2048]{1,0:T(8,128)(2,1)} %all-gather.6.cloned.1.call-done, bf16[2048,2112]{0,1:T(8,128)(2,1)} %all-gather.8.cloned.1.call-done), kind=kOutput, calls=%fused_computation.17 | convolution fusion | flops 4430266368 | bytes 11075584 | tf_op jit(solution)/shard_map/dot_general | solution.py:131
  280.9 3.2 collective-permute-start
  284.1 1.3 collective-permute-start.1
  285.6 2.9 collective-permute-done.1
  288.5 0.4 maximum_convert_fusion
  288.9 1.3 fusion.7
  290.2 5.1 %convolution_convert_fusion = bf16[768,2048]{1,0:T(8,128)(2,1)S(1)} fusion(bf16[2048,2112]{0,1:T(8,128)(2,1)} %all-gather.8.cloned.1.call-done, f32[768,1408]{1,0:T(8,128)S(1)} %fusion.7), kind=kOutput, calls=%fused_computation.15 | convolution fusion | flops 2221572096 | bytes 10747904 | tf_op jit(solution)/shard_map/dot_general | solution.py:143
  295.3 42.0 %all_to_all.11 = bf16[8,96,2048]{2,1,0:T(8,128)(2,1)S(1)} all-to-all(bf16[8,96,2048]{2,1,0:T(8,128)(2,1)S(1)} %bitcast.15), channel_id=1, replica_groups=mesh['grp'=2,'sp'=16,'tp'=8] {'tp'}, dimensions={0} | all-to-all | bytes 6291456 | tf_op jit(solution)/shard_map/all_to_all | solution.py:29
  337.3 0.6 convert_reduce_fusion
  337.9 0.8 fusion.47
  (38 shorter events, 0.5 us)
Async XLA Ops:
  6.5 134.7 %copy-start = (bf16[128,2048]{1,0:T(8,128)(2,1)S(1)}, bf16[128,2048]{1,0:T(8,128)(2,1)}, u32[]{:S(2)}) copy-start(bf16[128,2048]{1,0:T(8,128)(2,1)} %param.20) | copy-start | bytes 1572868
  6.6 4.0 %copy-start.3 = (bf16[768,256]{1,0:T(8,128)(2,1)S(1)}, bf16[768,256]{1,0:T(8,128)(2,1)}, u32[]{:S(2)}) copy-start(bf16[768,256]{1,0:T(8,128)(2,1)} %param.15) | copy-start | bytes 1179652
  6.6 4.0 %copy-start.10 = (f32[128]{0:T(128)S(1)}, f32[128]{0:T(128)}, u32[]{:S(2)}) copy-start(f32[128]{0:T(128)} %param.18) | copy-start | bytes 1540
  6.6 103.0 %all-gather.4.cloned.1.call-start = ((), (), s32[]{:S(2)}) async-start(), calls=%async_computation.2 | async-start | bytes 6684672 | tf_op jit(solution)/shard_map/all_gather | solution.py:15
  8.9 6.6 %copy-start.2 = (bf16[768,128]{1,0:T(8,128)(2,1)S(1)}, bf16[768,128]{1,0:T(8,128)(2,1)}, u32[]{:S(2)}) copy-start(bf16[768,128]{1,0:T(8,128)(2,1)} %param.14) | copy-start | bytes 589828
  8.9 6.8 %copy-start.9 = (f32[128]{0:T(128)S(1)}, f32[128]{0:T(128)}, u32[]{:S(2)}) copy-start(f32[128]{0:T(128)} %param.17) | copy-start | bytes 1540
  13.4 216.8 %all-gather.8.cloned.1.call-start = ((), (), s32[]{:S(2)}) async-start(), calls=%async_computation.4 | async-start | bytes 9191424 | tf_op jit(solution)/shard_map/all_gather | solution.py:15
  15.5 257.0 %all-gather.6.cloned.1.call-start = ((), (), s32[]{:S(2)}) async-start(), calls=%async_computation.3 | async-start | bytes 3538944 | tf_op jit(solution)/shard_map/all_gather | solution.py:132
  159.9 46.4 %copy-start.4 = (bf16[96,2048]{1,0:T(8,128)(2,1)S(1)}, bf16[96,2048]{1,0:T(8,128)(2,1)}, u32[]{:S(2)}) copy-start(bf16[96,2048]{1,0:T(8,128)(2,1)} %param.19) | copy-start | bytes 1179652
  159.9 46.4 %copy-start.7 = (f32[2048]{0:T(1024)S(1)}, f32[2048]{0:T(1024)}, u32[]{:S(2)}) copy-start(f32[2048]{0:T(1024)} %param.21) | copy-start | bytes 24580
  205.6 1.1 copy-start.8
  207.7 77.8 %copy-start.5 = (f32[3,704]{1,0:T(4,128)S(1)}, f32[3,704]{1,0:T(4,128)}, u32[]{:S(2)}) copy-start(f32[3,704]{1,0:T(4,128)} %param.26) | copy-start | bytes 25348
  207.7 77.8 %copy-start.6 = (f32[3,704]{1,0:T(4,128)S(1)}, f32[3,704]{1,0:T(4,128)}, u32[]{:S(2)}) copy-start(f32[3,704]{1,0:T(4,128)} %param.25) | copy-start | bytes 25348
  280.9 4.6 %collective-permute-start = (bf16[1,1408]{1,0:T(2,128)(2,1)S(1)}, bf16[1,1408]{1,0:T(2,128)(2,1)S(1)}, u32[]{:S(2)}, u32[]{:S(2)}) collective-permute-start(bf16[1,1408]{1,0:T(2,128)(2,1)S(1)} %get-tuple-element.10), channel_id=1, source_target_pairs={{0,8},{8,16},{16,24},{24,32},{32,40},{40,48},{48,56},{56,64},{64,7... | collective-permute-start | bytes 8456 | tf_op jit(solution)/shard_map/ppermute | solution.py:38
  284.1 4.4 %collective-permute-start.1 = (bf16[1,1408]{1,0:T(2,128)(2,1)S(1)}, bf16[1,1408]{1,0:T(2,128)(2,1)S(1)}, u32[]{:S(2)}, u32[]{:S(2)}) collective-permute-start(bf16[1,1408]{1,0:T(2,128)(2,1)S(1)} %get-tuple-element.11), channel_id=1, source_target_pairs={{8,0},{16,8},{24,16},{32,24},{40,32},{48,40},{56,48},{64,56},{72,6... | collective-permute-start | bytes 8456 | tf_op jit(solution)/shard_map/ppermute | solution.py:41
  295.3 43.4 %copy-start.1 = (bf16[128,2048]{1,0:T(8,128)(2,1)S(1)}, bf16[128,2048]{1,0:T(8,128)(2,1)}, u32[]{:S(2)}) copy-start(bf16[128,2048]{1,0:T(8,128)(2,1)} %param.20) | copy-start | bytes 1572868
Sparse Core Ops, SparseCore 0:
  13.5 95.9 all-gather.3
  111.3 118.8 all-gather.7
  232.0 40.3 all-gather.5
where the time goes:
time: 346 us; the launch traced here: 345 us
  waiting for transfers between devices  161 us (47%)
  blocking collectives  87.7 us (25%)
  matrix products  48.5 us (14%)
  other arithmetic  28.9 us (8%)
  between operations  13.4 us (4%)
  starting transfers between devices  4.63 us (1%)
    all_gather x2, waiting for transfers between devices, sent_together(): lax.all_gather(both, axis, axis=dim, tiled=True)  116 us
    all_to_all x2, blocking collectives, summed_on_arrival(): lax.all_to_all(tiles, axis, split_axis=0, concat_axis=0, tiled=True)  87.7 us
    all_gather x1, waiting for transfers between devices, body(): lax.all_gather(normed, 'tp', axis=0, tiled=True)  42.3 us
    dot_general x1, matrix products, body(): jnp.dot(block_rows, out_weight, preferred_element_type=jnp.float32)  18.7 us
    dot_general x1, matrix products, body(): lax.dot_general(query_rows, key_piece, (((1,), (1,)), ((), ())), preferre...  16.3 us
    reduce_sum x1, other arithmetic, body(): denom = jnp.sum(weights, axis=1, keepdims=True)  15.4 us
    dot_general x1, matrix products, body(): jnp.dot(lax.all_gather(normed, 'tp', axis=0, tiled=True), paired, preferr...  8.42 us
  transfers between devices with their start and end apart: 5, of which 4 were waited for; matrix products, arithmetic and copies ran while one was open for 16% of the time, Pallas kernels for 0%

commit v1 on v0

--- a/solution.py
+++ b/solution.py
@@ -8,6 +8,14 @@
 GRID_W = 64
 EPSILON = 1e-06
 THETA = 10000.0
+
+
+def gather_from_all(shard, axis, dim):
+    peers = lax.axis_size(axis)
+    repeats = [peers if d == dim else 1 for d in range(shard.ndim)]
+    return lax.all_to_all(
+        jnp.tile(shard, repeats), axis, split_axis=dim, concat_axis=dim, tiled=True
+    )
 
 
 def sent_together(arrays, axis, dim, along):
@@ -129,7 +137,7 @@
     normed = rms_rows(stream, ffn_gain).astype(jnp.bfloat16)
     paired = jnp.concatenate([gate_rows, value_rows], axis=1)
     upward = jnp.dot(
-        lax.all_gather(normed, "tp", axis=0, tiled=True), paired, preferred_element_type=jnp.float32
+        gather_from_all(normed, "tp", 0), paired, preferred_element_type=jnp.float32
     ).astype(jnp.bfloat16)
     padded = with_halo(upward, (("sp", 0),), 1).astype(jnp.float32)
     taps = jnp.concatenate([conv_gate, conv_value], axis=1)

time: 346 us -> 325 us (0.939)
  waiting for transfers between devices: 161 us -> 134 us
  starting transfers between devices: 4.63 us -> 8.99 us
    all_gather x1 -> x0, waiting for transfers between devices: 42.3 us -> none  [body(): lax.all_gather(normed, 'tp', axis=0, tiled=True)]
    all_to_all x0 -> x1, waiting for transfers between devices: none -> 21.7 us  [gather_from_all(): lax.all_to_all(jnp.tile(shard, repeats), axis, split_axis=dim, concat_axi...]
    all_gather x2, waiting for transfers between devices: 116 us -> 109 us  [sent_together(): lax.all_gather(both, axis, axis=dim, tiled=True)]
    all_to_all x0 -> x1, starting transfers between devices: none -> 5.31 us  [gather_from_all(): lax.all_to_all(jnp.tile(shard, repeats), axis, split_axis=dim, concat_axi...]
  transfers between devices with their start and end apart: 5 -> 5, of which waited for: 4 -> 4; matrix products, arithmetic and copies ran while one was open for 16% -> 17% of each run, Pallas kernels for 0% -> 0%
where the time goes in v1:
time: 325 us
  waiting for transfers between devices  134 us (41%)
  blocking collectives  88.2 us (27%)
  matrix products  48.5 us (15%)
  other arithmetic  28.1 us (9%)
  between operations  13.7 us (4%)
  starting transfers between devices  8.99 us (3%)
    all_gather x2, waiting for transfers between devices, sent_together(): lax.all_gather(both, axis, axis=dim, tiled=True)  109 us
    all_to_all x2, blocking collectives, summed_on_arrival(): lax.all_to_all(tiles, axis, split_axis=0, concat_axis=0, tiled=True)  88.2 us
    all_to_all x1, waiting for transfers between devices, gather_from_all(): lax.all_to_all(jnp.tile(shard, repeats), axis, split_axis=dim, concat_axi...  21.7 us
    dot_general x1, matrix products, body(): jnp.dot(block_rows, out_weight, preferred_element_type=jnp.float32)  18.7 us
    dot_general x1, matrix products, body(): lax.dot_general(query_rows, key_piece, (((1,), (1,)), ((), ())), preferre...  16.3 us
    reduce_sum x1, other arithmetic, body(): denom = jnp.sum(weights, axis=1, keepdims=True)  15.4 us
    dot_general x1, matrix products, body(): jnp.dot(gather_from_all(normed, 'tp', 0), paired, preferred_element_type=...  8.44 us
  transfers between devices with their start and end apart: 5, of which 4 were waited for; matrix products, arithmetic and copies ran while one was open for 17% of the time, Pallas kernels for 0%

profile of v1, /device:TPU:33, one launch (start us, length us, event | category | flops | bytes accessed | tf_op | source)
XLA Modules:
  0.0 324.6 jit_solution(421767401948182054)
XLA Ops:
  6.6 1.2 fusion.55
  7.8 1.1 fusion.56
  8.9 0.4 slice_negate_fusion.1
  9.3 0.9 constant_dynamic-slice_fusion
  10.3 0.3 broadcast_multiply_fusion.1
  10.6 2.0 fusion.60
  12.6 0.8 pad_maximum_fusion.2
  13.5 1.9 pad_maximum_fusion
  15.5 0.2 fusion.48
  15.7 0.2 fusion.50
  15.9 0.4 fusion.58
  16.3 93.3 %all-gather.3.cloned.1.call-done = bf16[12288,256]{1,0:T(8,128)(2,1)} async-done(((bf16[768,256]{1,0:T(8,128)(2,1)}), bf16[12288,256]{1,0:T(8,128)(2,1)}) %all-gather.3.cloned.1.call-update) | async-done | bytes 6291472 | tf_op jit(solution)/shard_map/all_gather | solution.py:23
  109.5 16.3 %fusion.87 = (f32[768]{0:T(1024)S(1)}, f32[768,12288]{1,0:T(8,128)}) fusion(bf16[12288,256]{1,0:T(8,128)(2,1)} %all-gather.3.cloned.1.call-done, bf16[768,128]{1,0:T(8,128)(2,1)S(1)} %copy-done.2, f32[768,32]{1,0:T(8,128)S(1)} %get-tuple-element.13, f32[768,32]{1,0:T(8,128)S(1)} %get-tuple-element.14, f32[768,32]{1,0:T(8,128)S(1)} %get-tuple-element.15, ...), kind=kOutput, calls=%fused_computation.117 | convolution fusion | flops 2426731776 | bytes 41687552 | tf_op jit(solution)/shard_map/dot_general | solution.py:120
  125.9 15.4 %fusion = f32[768]{0:T(1024)S(1)} fusion(f32[768,12288]{1,0:T(8,128)} %get-tuple-element.23, f32[768]{0:T(1024)S(1)} %broadcast_maximum_fusion), kind=kLoop, calls=%fused_computation.1 | loop fusion | flops 18873600 | bytes 37754880 | tf_op jit(solution)/shard_map/reduce_sum | solution.py:125
  141.2 18.7 %convolution_convert_fusion.1 = bf16[768,2048]{1,0:T(8,128)(2,1)} fusion(bf16[128,2048]{1,0:T(8,128)(2,1)S(1)} %copy-done, bf16[12288,256]{1,0:T(8,128)(2,1)} %all-gather.3.cloned.1.call-done, f32[768,12288]{1,0:T(8,128)} %get-tuple-element.23, f32[768]{0:T(1024)S(1)} %broadcast_maximum_fusion, f32[768]{0:T(1024)S(1)} %fusion), kind=kOutput, calls=%fused_computation.16 | convolution fusion | flops 2839216128 | bytes 44570624 | tf_op jit(solution)/shard_map/dot_general | solution.py:132
  159.9 45.7 %all_to_all.19 = bf16[8,96,2048]{2,1,0:T(8,128)(2,1)S(1)} all-to-all(bf16[8,96,2048]{2,1,0:T(8,128)(2,1)} %bitcast.15), channel_id=1, replica_groups=mesh['grp'=2,'sp'=16,'tp'=8] {'tp'}, dimensions={0} | all-to-all | bytes 6291456 | tf_op jit(solution)/shard_map/all_to_all | solution.py:37
  205.6 0.6 convert_reduce_fusion.1
  206.3 0.3 fusion.44
  206.9 2.1 tile.2
  209.0 5.3 %all-to-all-start.1 = ((bf16[8,96,2048]{2,1,0:T(8,128)(2,1)}), bf16[8,96,2048]{2,1,0:T(8,128)(2,1)}, u32[]{:S(2)}, u32[]{:S(2)}) async-start(bf16[8,96,2048]{2,1,0:T(8,128)(2,1)} %tile.2), calls=%async_computation.1 | async-start | bytes 6291456 | tf_op jit(solution)/shard_map/all_to_all | solution.py:16
  214.3 15.9 %all-gather.5.cloned.1.call-done = bf16[2048,2112]{0,1:T(8,128)(2,1)} async-done(((bf16[128,2112]{0,1:T(8,128)(2,1)}), bf16[2048,2112]{0,1:T(8,128)(2,1)}) %all-gather.5.cloned.1.call-update) | async-done | bytes 8650768 | tf_op jit(solution)/shard_map/all_gather | solution.py:23
  230.2 21.7 %all-to-all-done.1 = bf16[8,96,2048]{2,1,0:T(8,128)(2,1)} async-done(((bf16[8,96,2048]{2,1,0:T(8,128)(2,1)}), bf16[8,96,2048]{2,1,0:T(8,128)(2,1)}, u32[]{:S(2)}, u32[]{:S(2)}) %all-to-all-start.1) | async-done | bytes 3145760 | tf_op jit(solution)/shard_map/all_to_all | solution.py:16
  251.9 8.4 %fusion.9 = bf16[768,1408]{1,0:T(8,128)(2,1)S(1)} fusion(bf16[768,2048]{1,0:T(8,128)(2,1)} %bitcast.6, bf16[2048,2112]{0,1:T(8,128)(2,1)} %all-gather.5.cloned.1.call-done), kind=kOutput, calls=%fused_computation.17 | convolution fusion | flops 4430266368 | bytes 11075584 | tf_op jit(solution)/shard_map/dot_general | solution.py:139
  260.4 2.3 collective-permute-start
  262.7 1.3 collective-permute-start.1
  264.1 2.9 collective-permute-done.1
  267.1 0.4 maximum_convert_fusion
  267.5 1.3 fusion.7
  268.8 5.1 %convolution_convert_fusion = bf16[768,2048]{1,0:T(8,128)(2,1)S(1)} fusion(bf16[2048,2112]{0,1:T(8,128)(2,1)} %all-gather.5.cloned.1.call-done, f32[768,1408]{1,0:T(8,128)S(1)} %fusion.7), kind=kOutput, calls=%fused_computation.15 | convolution fusion | flops 2221572096 | bytes 10747904 | tf_op jit(solution)/shard_map/dot_general | solution.py:151
  273.9 42.5 %all_to_all.20 = bf16[8,96,2048]{2,1,0:T(8,128)(2,1)S(1)} all-to-all(bf16[8,96,2048]{2,1,0:T(8,128)(2,1)S(1)} %bitcast.16), channel_id=1, replica_groups=mesh['grp'=2,'sp'=16,'tp'=8] {'tp'}, dimensions={0} | all-to-all | bytes 6291456 | tf_op jit(solution)/shard_map/all_to_all | solution.py:37
  316.4 0.6 convert_reduce_fusion
  316.9 0.8 fusion.47
  (38 shorter events, 0.7 us)
Async XLA Ops:
  6.5 134.7 %copy-start = (bf16[128,2048]{1,0:T(8,128)(2,1)S(1)}, bf16[128,2048]{1,0:T(8,128)(2,1)}, u32[]{:S(2)}) copy-start(bf16[128,2048]{1,0:T(8,128)(2,1)} %param.20) | copy-start | bytes 1572868
  6.6 4.0 %copy-start.3 = (bf16[768,256]{1,0:T(8,128)(2,1)S(1)}, bf16[768,256]{1,0:T(8,128)(2,1)}, u32[]{:S(2)}) copy-start(bf16[768,256]{1,0:T(8,128)(2,1)} %param.15) | copy-start | bytes 1179652
  6.6 4.0 %copy-start.10 = (f32[128]{0:T(128)S(1)}, f32[128]{0:T(128)}, u32[]{:S(2)}) copy-start(f32[128]{0:T(128)} %param.18) | copy-start | bytes 1540
  6.6 103.0 %all-gather.3.cloned.1.call-start = ((), (), s32[]{:S(2)}) async-start(), calls=%async_computation.3 | async-start | bytes 6684672 | tf_op jit(solution)/shard_map/all_gather | solution.py:23
  8.9 6.6 %copy-start.2 = (bf16[768,128]{1,0:T(8,128)(2,1)S(1)}, bf16[768,128]{1,0:T(8,128)(2,1)}, u32[]{:S(2)}) copy-start(bf16[768,128]{1,0:T(8,128)(2,1)} %param.14) | copy-start | bytes 589828
  8.9 6.8 %copy-start.9 = (f32[128]{0:T(128)S(1)}, f32[128]{0:T(128)}, u32[]{:S(2)}) copy-start(f32[128]{0:T(128)} %param.17) | copy-start | bytes 1540
  13.4 216.8 %all-gather.5.cloned.1.call-start = ((), (), s32[]{:S(2)}) async-start(), calls=%async_computation.4 | async-start | bytes 9191424 | tf_op jit(solution)/shard_map/all_gather | solution.py:23
  159.9 46.4 %copy-start.4 = (bf16[96,2048]{1,0:T(8,128)(2,1)S(1)}, bf16[96,2048]{1,0:T(8,128)(2,1)}, u32[]{:S(2)}) copy-start(bf16[96,2048]{1,0:T(8,128)(2,1)} %param.19) | copy-start | bytes 1179652
  159.9 46.4 %copy-start.7 = (f32[2048]{0:T(1024)S(1)}, f32[2048]{0:T(1024)}, u32[]{:S(2)}) copy-start(f32[2048]{0:T(1024)} %param.21) | copy-start | bytes 24580
  205.6 1.1 copy-start.8
  209.0 42.9 %all-to-all-start.1 = ((bf16[8,96,2048]{2,1,0:T(8,128)(2,1)}), bf16[8,96,2048]{2,1,0:T(8,128)(2,1)}, u32[]{:S(2)}, u32[]{:S(2)}) async-start(bf16[8,96,2048]{2,1,0:T(8,128)(2,1)} %tile.2), calls=%async_computation.1 | async-start | bytes 6291456 | tf_op jit(solution)/shard_map/all_to_all | solution.py:16
  251.9 12.1 %copy-start.5 = (f32[3,704]{1,0:T(4,128)S(1)}, f32[3,704]{1,0:T(4,128)}, u32[]{:S(2)}) copy-start(f32[3,704]{1,0:T(4,128)} %param.26) | copy-start | bytes 25348
  251.9 12.1 %copy-start.6 = (f32[3,704]{1,0:T(4,128)S(1)}, f32[3,704]{1,0:T(4,128)}, u32[]{:S(2)}) copy-start(f32[3,704]{1,0:T(4,128)} %param.25) | copy-start | bytes 25348
  260.4 3.8 %collective-permute-start = (bf16[1,1408]{1,0:T(2,128)(2,1)S(1)}, bf16[1,1408]{1,0:T(2,128)(2,1)S(1)}, u32[]{:S(2)}, u32[]{:S(2)}) collective-permute-start(bf16[1,1408]{1,0:T(2,128)(2,1)S(1)} %get-tuple-element.10), channel_id=1, source_target_pairs={{0,8},{8,16},{16,24},{24,32},{32,40},{40,48},{48,56},{56,64},{64,7... | collective-permute-start | bytes 8456 | tf_op jit(solution)/shard_map/ppermute | solution.py:46
  262.7 4.4 %collective-permute-start.1 = (bf16[1,1408]{1,0:T(2,128)(2,1)S(1)}, bf16[1,1408]{1,0:T(2,128)(2,1)S(1)}, u32[]{:S(2)}, u32[]{:S(2)}) collective-permute-start(bf16[1,1408]{1,0:T(2,128)(2,1)S(1)} %get-tuple-element.11), channel_id=1, source_target_pairs={{8,0},{16,8},{24,16},{32,24},{40,32},{48,40},{56,48},{64,56},{72,6... | collective-permute-start | bytes 8456 | tf_op jit(solution)/shard_map/ppermute | solution.py:49
  273.9 43.9 %copy-start.1 = (bf16[128,2048]{1,0:T(8,128)(2,1)S(1)}, bf16[128,2048]{1,0:T(8,128)(2,1)}, u32[]{:S(2)}) copy-start(bf16[128,2048]{1,0:T(8,128)(2,1)} %param.20) | copy-start | bytes 1572868
Sparse Core Ops, SparseCore 0:
  13.5 95.9 all-gather.2
  111.3 118.8 all-gather.4
